TPU v7x, 32 devices: a whole 2x2x4 slice. The times are simulated.
32 devices in a mesh: grp: 2 (over y), sp: 4 (over z), tp: 4 (over x, core).
Axes of the slice: x: 2, y: 2, z: 4, core: 2. Of those that a mesh axis runs over, the one named last changes fastest.
Arguments:
- resid_in: bfloat16 [2048, 2048], P(('grp', 'sp', 'tp')), parts along dimension 0, may hold values from -6 to 6
- query_narrow: bfloat16 [2048, 8, 128], P(('grp', 'sp'), 'tp'), parts along dimension 0, may hold values from -512 to 512
- key_narrow: bfloat16 [2048, 4, 128], P(('grp', 'sp'), 'tp'), parts along dimension 0, may hold values from -512 to 512
- value_narrow: bfloat16 [2048, 4, 128], P(('grp', 'sp'), 'tp'), parts along dimension 0, may hold values from -6 to 6
- query_wide: bfloat16 [2048, 8, 256], P(('grp', 'sp'), 'tp'), parts along dimension 0, may hold values from -512 to 512
- key_wide: bfloat16 [2048, 4, 256], P(('grp', 'sp'), 'tp'), parts along dimension 0, may hold values from -512 to 512
- value_wide: bfloat16 [2048, 4, 128], P(('grp', 'sp'), 'tp'), parts along dimension 0, may hold values from -6 to 6
- lambda_narrow: float32 [8], P('tp'), may hold values from 0.3 to 0.8
- lambda_wide: float32 [8], P('tp'), may hold values from 0.3 to 0.8
- head_gain: float32 [128], replicated, may hold values from 0.1 to 1.9
- out_narrow: bfloat16 [1024, 2048], P('tp'), may hold values from -0.125 to 0.125
- out_wide: bfloat16 [1024, 2048], P('tp'), may hold values from -0.125 to 0.125
- norm_gain: bfloat16 [2048], replicated, may hold values from 0.099609375 to 1.8984375
- up_weight: bfloat16 [2048, 8192], P('sp', 'tp'), may hold values from -0.125 to 0.125
- down_weight: bfloat16 [8192, 2048], P('tp', 'sp'), may hold values from -0.0625 to 0.0625
Outputs:
- mixed_out: bfloat16 [2048, 2048], P(('grp', 'sp', 'tp')), parts along dimension 0
There are 2 independent parts, one for each index of `grp`. A program takes and returns all parts, laid end to end along the dimension named above; an argument that names none is the same for every part. Nothing has to cross between parts.
All inputs are finite; a program needn't handle non-finite values.
Results may differ from a plain program's by a relative error of at most 0.018.
Values may be sent and summed in bfloat16 or wider, within the bound.
A program may use at most 128 MiB of HBM per device.

v0:
```python
import math
import jax
import jax.numpy as jnp
from jax import lax
from jax.sharding import PartitionSpec as P

NORM_EPS = 1e-06
OUT_SCALE = 0.8


def empty_state(query, key_head_stack, value_width):
    row_count, head_count = (query.shape[0], query.shape[1])
    group_size = head_count // key_head_stack
    row_top = jnp.full((key_head_stack, group_size, 2, row_count), -jnp.inf, jnp.float32)
    row_total = jnp.zeros((key_head_stack, group_size, 2, row_count), jnp.float32)
    weighted_values = jnp.zeros(
        (key_head_stack, group_size, 2, row_count, value_width), jnp.float32
    )
    return (row_top, row_total, weighted_values)


def absorb(states, query, key_rows, values):
    row_count, head_count = (query.shape[0], query.shape[1])
    key_head_stack = key_rows.shape[1]
    half_width = key_rows.shape[2] // 2
    group_size = head_count // key_head_stack
    value_width = values.shape[2]
    amount = key_rows.shape[0]
    block_rows = math.gcd(amount, 512)
    rotation_count = amount // block_rows
    grouped = query.reshape(row_count, key_head_stack, group_size, 2, half_width)
    key_block_list = key_rows.reshape(rotation_count, block_rows, key_head_stack, 2, half_width)
    value_blocks = values.reshape(rotation_count, block_rows, key_head_stack, value_width)

    def visit(running, kv_pair):
        row_top, row_total, weighted_values = running
        key_blk, value_blk = kv_pair
        scores = jnp.einsum(
            "tkgcd,skcd->kgcts", grouped, key_blk, preferred_element_type=jnp.float32
        ) * half_width ** (-0.5)
        new_top = jnp.maximum(row_top, jnp.max(scores, axis=-1))
        rescale = jnp.exp(row_top - new_top)
        powers = jnp.exp(scores - new_top[..., None])
        row_total = row_total * rescale + jnp.sum(powers, axis=-1)
        weighted_values = weighted_values * rescale[..., None] + jnp.einsum(
            "iodph,hie->iodpe",
            powers.astype(jnp.bfloat16),
            value_blk,
            preferred_element_type=jnp.float32,
        )
        return ((new_top, row_total, weighted_values), None)

    outcome, _ = lax.scan(visit, states, (key_block_list, value_blocks))
    return outcome


def finish(states, lambdas, gain_vec):
    row_top, row_total, weighted_values = states
    key_head_stack, group_size, row_count = (row_top.shape[0], row_top.shape[1], row_top.shape[3])
    value_width = weighted_values.shape[4]
    first_map = weighted_values[:, :, 0] / row_total[:, :, 0, :, None]
    second_map = weighted_values[:, :, 1] / row_total[:, :, 1, :, None]
    mixed = first_map - lambdas.reshape(key_head_stack, group_size)[:, :, None, None] * second_map
    normed = (
        mixed
        * lax.rsqrt(jnp.mean(mixed * mixed, axis=-1, keepdims=True) + NORM_EPS)
        * gain_vec
        * OUT_SCALE
    )
    normed = normed.astype(jnp.bfloat16).transpose(2, 0, 1, 3)
    return normed.reshape(row_count, key_head_stack * group_size * value_width)


def attend(
    query_narrow,
    key_narrow,
    value_narrow,
    query_wide,
    key_wide,
    value_wide,
    lambda_narrow,
    lambda_wide,
    head_gain,
):
    initial = (
        empty_state(query_narrow, key_narrow.shape[1], value_narrow.shape[2]),
        empty_state(query_wide, key_wide.shape[1], value_wide.shape[2]),
    )
    narrow_keys = lax.all_gather(key_narrow, "sp", axis=0, tiled=True)
    narrow_values = lax.all_gather(value_narrow, "sp", axis=0, tiled=True)
    wide_keys = lax.all_gather(key_wide, "sp", axis=0, tiled=True)
    wide_values = lax.all_gather(value_wide, "sp", axis=0, tiled=True)
    narrow_state = absorb(initial[0], query_narrow, narrow_keys, narrow_values)
    wide_state = absorb(initial[1], query_wide, wide_keys, wide_values)
    return (
        finish(narrow_state, lambda_narrow, head_gain),
        finish(wide_state, lambda_wide, head_gain),
    )


def shards(
    resid_in,
    query_narrow,
    key_narrow,
    value_narrow,
    query_wide,
    key_wide,
    value_wide,
    lambda_narrow,
    lambda_wide,
    head_gain,
    out_narrow,
    out_wide,
    norm_gain,
    up_weight,
    down_weight,
):
    att_narrow, att_wide = attend(
        query_narrow,
        key_narrow,
        value_narrow,
        query_wide,
        key_wide,
        value_wide,
        lambda_narrow,
        lambda_wide,
        head_gain,
    )
    projected = lax.psum_scatter(
        (
            jnp.dot(att_narrow, out_narrow, preferred_element_type=jnp.float32)
            + jnp.dot(att_wide, out_wide, preferred_element_type=jnp.float32)
        ).astype(jnp.bfloat16),
        "tp",
        scatter_dimension=0,
        tiled=True,
    ).astype(jnp.float32)
    middle = (resid_in.astype(jnp.float32) + projected).astype(jnp.bfloat16)
    middle_f32 = middle.astype(jnp.float32)
    normed = middle_f32 * lax.rsqrt(
        jnp.mean(middle_f32 * middle_f32, axis=-1, keepdims=True) + NORM_EPS
    )
    normed = (normed * norm_gain.astype(jnp.float32)).astype(jnp.bfloat16)
    whole_rows = lax.all_gather(normed, "tp", axis=0, tiled=True)
    up_collected = lax.all_gather(up_weight, "sp", axis=0, tiled=True)
    lifted = jnp.dot(whole_rows, up_collected, preferred_element_type=jnp.float32)
    activated = jnp.square(jax.nn.relu(lifted)).astype(jnp.bfloat16)
    partials = jnp.dot(
        activated,
        lax.all_gather(down_weight, "sp", axis=1, tiled=True),
        preferred_element_type=jnp.float32,
    )
    mixer_out = lax.psum_scatter(
        partials.astype(jnp.bfloat16), "tp", scatter_dimension=0, tiled=True
    ).astype(jnp.float32)
    return (middle_f32 + mixer_out).astype(jnp.bfloat16)


def solution(mesh):
    placed = (
        P(("grp", "sp", "tp"), None),
        P(("grp", "sp"), "tp", None),
        P(("grp", "sp"), "tp", None),
        P(("grp", "sp"), "tp", None),
        P(("grp", "sp"), "tp", None),
        P(("grp", "sp"), "tp", None),
        P(("grp", "sp"), "tp", None),
        P("tp"),
        P("tp"),
        P(),
        P("tp", None),
        P("tp", None),
        P(),
        P("sp", "tp"),
        P("tp", "sp"),
    )
    return jax.shard_map(
        shards, mesh=mesh, in_specs=placed, out_specs=P(("grp", "sp", "tp"), None), check_vma=False
    )
```

profile of v0, /device:TPU:0, one launch (start us, length us, event | category | flops | bytes accessed | tf_op | source)
XLA Modules:
  0.0 480.9 jit_solution(12649065433829812458)
XLA Ops:
  6.6 17.7 %all_gather.23 = bf16[1024,1,256]{2,0,1:T(8,128)(2,1)S(1)} all-gather(bf16[256,1,256]{2,0,1:T(8,128)(2,1)} %param.24), channel_id=1, replica_groups=mesh['grp'=2,'sp'=4,'tp'=4] {'sp'}, dimensions={0}, use_global_device_ids=true | all-gather | bytes 655360 | tf_op jit(solution)/shard_map/all_gather | solution.py:91
  24.3 0.1 reshape.256
  24.4 1.1 copy.33
  25.5 0.2 copy.35
  25.7 15.3 %all_gather.24 = bf16[1024,1,128]{2,0,1:T(8,128)(2,1)} all-gather(bf16[256,1,128]{2,0,1:T(8,128)(2,1)S(1)} %copy-done.9), channel_id=1, replica_groups=mesh['grp'=2,'sp'=4,'tp'=4] {'sp'}, dimensions={0}, use_global_device_ids=true | all-gather | bytes 327680 | tf_op jit(solution)/shard_map/all_gather | solution.py:92
  41.1 8.2 %while.31 = (s32[]{:T(128)}, f32[1,2,2,256]{3,1,2,0:T(2,128)S(1)}, f32[1,2,2,256]{3,1,2,0:T(2,128)S(1)}, f32[1,2,2,256,128]{4,3,2,1,0:T(8,128)}, bf16[2,512,1,2,...) while((s32[]{:T(128)}, f32[1,2,2,256]{3,1,2,0:T(2,128)S(1)}, ...), condition=%wide.region_8.9_spmd.clone, body=%wide.region_5.0_spmd.clone.sunk | while | flops 271980544 | bytes 13832389 | solution.py:53
  41.1 0.2 constant_dynamic-slice_fusion.2
  41.3 0.6 copy-done.1
  41.9 0.4 bitcast_reduce_fusion.5
  42.4 0.4 fusion.71
  42.8 0.5 copy-done.7
  43.3 1.3 fusion.72
  44.7 0.2 constant_dynamic-slice_fusion.2
  44.9 0.6 copy-done.1
  45.5 0.4 bitcast_reduce_fusion.5
  46.0 0.4 fusion.71
  46.4 0.5 copy-done.7
  46.9 2.3 fusion.72
  49.3 0.0 copy-start.8
  49.3 0.6 slice_bitcast_fusion.5
  49.9 14.2 %all_gather.21 = bf16[1024,1,128]{2,0,1:T(8,128)(2,1)S(1)} all-gather(bf16[256,1,128]{2,0,1:T(8,128)(2,1)S(1)} %copy-done.10), channel_id=1, replica_groups=mesh['grp'=2,'sp'=4,'tp'=4] {'sp'}, dimensions={0}, use_global_device_ids=true | all-gather | bytes 327680 | tf_op jit(solution)/shard_map/all_gather | solution.py:89
  64.1 0.2 reshape.272
  64.3 0.4 copy.29
  64.7 15.6 %all_gather.22 = bf16[1024,1,128]{2,0,1:T(8,128)(2,1)} all-gather(bf16[256,1,128]{2,0,1:T(8,128)(2,1)} %param.22), channel_id=1, replica_groups=mesh['grp'=2,'sp'=4,'tp'=4] {'sp'}, dimensions={0}, use_global_device_ids=true | all-gather | bytes 327680 | tf_op jit(solution)/shard_map/all_gather | solution.py:90
  80.4 0.1 copy.28
  80.5 6.6 %while.30 = (s32[]{:T(128)}, f32[1,2,2,256]{3,1,2,0:T(2,128)S(1)}, f32[1,2,2,256]{3,1,2,0:T(2,128)S(1)}, f32[1,2,2,256,128]{4,3,2,1,0:T(8,128)}, bf16[2,512,1,2,...) while((s32[]{:T(128)}, f32[1,2,2,256]{3,1,2,0:T(2,128)S(1)}, ...), condition=%wide.region_3.4_spmd.clone, body=%wide.region_0.3_spmd.clone.sunk | while | flops 204871680 | bytes 8851597 | solution.py:53
  80.5 0.5 bitcast_reduce_fusion.4
  81.1 0.4 fusion.66
  81.5 0.5 copy-done.6
  82.0 1.3 fusion.67
  83.3 0.5 bitcast_reduce_fusion.4
  83.9 0.4 fusion.66
  84.3 0.5 copy-done.6
  84.8 2.3 fusion.67
  87.2 0.0 copy-start.11
  87.2 0.0 copy-start.13
  87.2 0.0 copy-start.14
  87.2 0.0 copy-start.15
  87.2 1.2 copy.36
  88.5 1.2 copy.31
  89.7 0.2 multiply_reduce_fusion
  89.9 0.0 copy-start.5
  90.0 0.1 multiply_convert_fusion
  90.1 0.5 fusion.45
  90.6 0.6 copy-done.5
  91.2 1.4 fusion.29
  92.6 0.0 reduce-scatter.3.cloned.1.call-update
  92.6 0.0 all-gather.4.cloned.1.call-start
  92.7 25.0 %reduce-scatter.3.cloned.1.call-done = bf16[64,2048]{1,0:T(8,128)(2,1)} async-done(((bf16[256,2048]{1,0:T(8,128)(2,1)}), bf16[64,2048]{1,0:T(8,128)(2,1)}) %reduce-scatter.3.cloned.1.call-update) | async-done | bytes 262160 | tf_op jit(solution)/shard_map/reduce_scatter | solution.py:129
  117.7 1.1 fusion.30
  118.8 1.8 fusion.32
  120.6 0.0 all-gather.4.cloned.1.call-update
  120.6 0.0 all-gather.6.cloned.1.call-start
  120.7 0.7 all-gather.6.cloned.1.call-update
  121.3 0.0 all-gather.8.cloned.1.call-start
  121.4 0.5 all-gather.8.cloned.1.call-update
  121.9 0.0 reduce-scatter.5.cloned.1.call-start
  122.0 15.5 %all-gather.4.cloned.1.call-done = bf16[256,2048]{1,0:T(8,128)(2,1)} async-done(((bf16[64,2048]{1,0:T(8,128)(2,1)}), bf16[256,2048]{1,0:T(8,128)(2,1)}) %all-gather.4.cloned.1.call-update) | async-done | bytes 1048592 | tf_op jit(solution)/shard_map/all_gather | solution.py:144
  137.4 151.2 %all-gather.6.cloned.1.call-done = bf16[2048,2048]{1,0:T(8,128)(2,1)} async-done(((bf16[512,2048]{1,0:T(8,128)(2,1)}), bf16[2048,2048]{1,0:T(8,128)(2,1)}) %all-gather.6.cloned.1.call-update) | async-done | bytes 8388624 | tf_op jit(solution)/shard_map/all_gather | solution.py:145
  288.7 149.3 %all-gather.8.cloned.1.call-done = bf16[2048,2048]{1,0:T(8,128)(2,1)} async-done(((bf16[2048,512]{1,0:T(8,128)(2,1)}), bf16[2048,2048]{1,0:T(8,128)(2,1)}) %all-gather.8.cloned.1.call-update) | async-done | bytes 8388624 | tf_op jit(solution)/shard_map/all_gather | solution.py:150
  437.9 11.5 %convolution_convert_fusion = bf16[256,2048]{1,0:T(8,128)(2,1)} fusion(bf16[2048,2048]{1,0:T(8,128)(2,1)} %all-gather.8.cloned.1.call-done, bf16[256,2048]{1,0:T(8,128)(2,1)} %all-gather.4.cloned.1.call-done, bf16[2048,2048]{1,0:T(8,128)(2,1)} %all-gather.6.cloned.1.call-done), kind=kOutput, calls=%fused_computation.52 | convolution fusion | flops 4297064448 | bytes 18874368 | tf_op jit(solution)/shard_map/dot_general | solution.py:148
  449.5 0.0 reduce-scatter.5.cloned.1.call-update
  449.5 23.1 %reduce-scatter.5.cloned.1.call-done = bf16[64,2048]{1,0:T(8,128)(2,1)} async-done(((bf16[256,2048]{1,0:T(8,128)(2,1)}), bf16[64,2048]{1,0:T(8,128)(2,1)}) %reduce-scatter.5.cloned.1.call-update) | async-done | bytes 262160 | tf_op jit(solution)/shard_map/reduce_scatter | solution.py:153
  472.6 1.7 fusion.33
  (56 shorter events, 0.2 us)
Async XLA Ops:
  6.5 83.6 %copy-start = (bf16[256,2048]{1,0:T(8,128)(2,1)S(1)}, bf16[256,2048]{1,0:T(8,128)(2,1)}, u32[]{:S(2)}) copy-start(bf16[256,2048]{1,0:T(8,128)(2,1)} %param.29) | copy-start | bytes 3145732
  6.5 19.2 %copy-start.9 = (bf16[256,1,128]{2,0,1:T(8,128)(2,1)S(1)}, bf16[256,1,128]{2,0,1:T(8,128)(2,1)}, u32[]{:S(2)}) copy-start(bf16[256,1,128]{2,0,1:T(8,128)(2,1)} %param.25) | copy-start | bytes 196612
  6.5 111.1 %reduce-scatter.3.cloned.1.call-start = ((), (), s32[]{:S(2)}) async-start(), calls=%async_computation.2 | async-start | bytes 1310720 | tf_op jit(solution)/shard_map/reduce_scatter | solution.py:129
  41.1 8.8 %copy-start.10 = (bf16[256,1,128]{2,0,1:T(8,128)(2,1)S(1)}, bf16[256,1,128]{2,0,1:T(8,128)(2,1)}, u32[]{:S(2)}) copy-start(bf16[256,1,128]{2,0,1:T(8,128)(2,1)} %param.21) | copy-start | bytes 196612
  41.1 0.8 copy-start.1
  42.4 1.0 copy-start.7
  42.8 1.8 copy-start.2
  44.7 0.8 copy-start.1
  45.9 1.0 copy-start.7
  46.4 2.9 copy-start.2
  49.3 31.1 %copy-start.8 = (bf16[256,2,128]{2,1,0:T(2,128)(2,1)S(1)}, bf16[256,2,128]{2,1,0:T(2,128)(2,1)}, u32[]{:S(2)}) copy-start(bf16[256,2,128]{2,1,0:T(2,128)(2,1)} %param.20) | copy-start | bytes 393220
  81.0 1.0 copy-start.6
  83.8 1.0 copy-start.6
  87.2 2.6 copy-start.11
  87.2 2.6 copy-start.13
  87.2 2.6 copy-start.14
  87.2 2.8 copy-start.15
  89.9 1.2 copy-start.5
  91.2 1.5 copy-start.12
  91.2 26.5 %copy-start.3 = (bf16[64,2048]{1,0:T(8,128)(2,1)S(1)}, bf16[64,2048]{1,0:T(8,128)(2,1)}, u32[]{:S(2)}) copy-start(bf16[64,2048]{1,0:T(8,128)(2,1)} %param.19) | copy-start | bytes 786436
  92.6 44.8 %all-gather.4.cloned.1.call-start = ((), (), s32[]{:S(2)}) async-start(), calls=%async_computation.3 | async-start | bytes 1310720 | tf_op jit(solution)/shard_map/all_gather | solution.py:144
  120.6 168.1 %all-gather.6.cloned.1.call-start = ((), (), s32[]{:S(2)}) async-start(), calls=%async_computation.4 | async-start | bytes 10485760 | tf_op jit(solution)/shard_map/all_gather | solution.py:145
  121.3 316.6 %all-gather.8.cloned.1.call-start = ((), (), s32[]{:S(2)}) async-start(), calls=%async_computation.5 | async-start | bytes 10485760 | tf_op jit(solution)/shard_map/all_gather | solution.py:150
  121.9 350.7 %copy-start.4 = (bf16[64,2048]{1,0:T(8,128)(2,1)S(1)}, bf16[64,2048]{1,0:T(8,128)(2,1)}, u32[]{:S(2)}) copy-start(bf16[64,2048]{1,0:T(8,128)(2,1)} %reduce-scatter.3.cloned.1.call-done) | copy-start | bytes 786436
  121.9 350.7 %reduce-scatter.5.cloned.1.call-start = ((), (), s32[]{:S(2)}) async-start(), calls=%async_computation.6 | async-start | bytes 1310720 | tf_op jit(solution)/shard_map/reduce_scatter | solution.py:153
Sparse Core Ops, SparseCore 0:
  92.7 24.8 reduce-scatter.2
  120.7 16.6 all-gather.3
  139.0 149.6 all-gather.5
  290.1 147.7 all-gather.7
  449.6 22.9 reduce-scatter.4
where the time goes:
time: 481 us
  waiting for transfers between devices  365 us (76%)
  blocking collectives  62.9 us (13%)
  matrix products  22.6 us (5%)
  between operations  13.4 us (3%)
  local copies, waits for them, and re-layouts  9.51 us (2%)
  other arithmetic  6.74 us (1%)
    all_gather x1, waiting for transfers between devices, shards(): up_collected = lax.all_gather(up_weight, 'sp', axis=0, tiled=True)  151 us
    all_gather x1, waiting for transfers between devices, shards(): lax.all_gather(down_weight, 'sp', axis=1, tiled=True)  149 us
    reduce_scatter x1, waiting for transfers between devices, shards(): lax.psum_scatter((jnp.dot(att_narrow, out_narrow, preferred_element_type=...  25 us
    reduce_scatter x1, waiting for transfers between devices, shards(): lax.psum_scatter(partials.astype(jnp.bfloat16), 'tp', scatter_dimension=0...  23.1 us
    all_gather x1, blocking collectives, attend(): wide_keys = lax.all_gather(key_wide, 'sp', axis=0, tiled=True)  17.7 us
    all_gather x1, blocking collectives, attend(): narrow_values = lax.all_gather(value_narrow, 'sp', axis=0, tiled=True)  15.6 us
    all_gather x1, waiting for transfers between devices, shards(): whole_rows = lax.all_gather(normed, 'tp', axis=0, tiled=True)  15.5 us
    all_gather x1, blocking collectives, attend(): wide_values = lax.all_gather(value_wide, 'sp', axis=0, tiled=True)  15.3 us
  transfers between devices with their start and end apart: 5, of which 5 were waited for; matrix products, arithmetic and copies ran while one was open for 0% of the time, Pallas kernels for 0%

commit v1 on v0

--- a/solution.py
+++ b/solution.py
@@ -142,7 +142,12 @@
     )
     normed = (normed * norm_gain.astype(jnp.float32)).astype(jnp.bfloat16)
     whole_rows = lax.all_gather(normed, "tp", axis=0, tiled=True)
-    up_collected = lax.all_gather(up_weight, "sp", axis=0, tiled=True)
+    ring = [up_weight]
+    for hop in range(3):
+        ring.append(lax.ppermute(ring[-1], "sp", [(dev, (dev + 1) % 4) for dev in range(4)]))
+    up_collected = jnp.roll(
+        jnp.concatenate(ring[::-1], axis=0), (lax.axis_index("sp") + 1) * ring[0].shape[0], axis=0
+    )
     lifted = jnp.dot(whole_rows, up_collected, preferred_element_type=jnp.float32)
     activated = jnp.square(jax.nn.relu(lifted)).astype(jnp.bfloat16)
     partials = jnp.dot(

time: 481 us -> 458 us (0.952)
  waiting for transfers between devices: 365 us -> 249 us
  starting transfers between devices: 0.16 us -> 72.7 us
  local copies, waits for them, and re-layouts: 9.51 us -> 29.7 us
    ppermute x0 -> x3, waiting for transfers between devices: none -> 200 us  [shards(): lax.ppermute(ring[-1], 'sp', [(dev, (dev + 1) % 4) for dev in range(4)])]
    all_gather x1 -> x0, waiting for transfers between devices: 151 us -> none  [shards(): up_collected = lax.all_gather(up_weight, 'sp', axis=0, tiled=True)]
    all_gather x1, waiting for transfers between devices: 149 us -> 0.01 us  [shards(): lax.all_gather(down_weight, 'sp', axis=1, tiled=True)]
    ppermute x0 -> x3, starting transfers between devices: none -> 72.6 us  [shards(): lax.ppermute(ring[-1], 'sp', [(dev, (dev + 1) % 4) for dev in range(4)])]
    unnamed x29 -> x42, local copies, waits for them, and re-layouts: 2.43 us -> 21.2 us
    all_gather x1, waiting for transfers between devices: 15.5 us -> 0.01 us  [shards(): whole_rows = lax.all_gather(normed, 'tp', axis=0, tiled=True)]
  transfers between devices with their start and end apart: 5 -> 7, of which waited for: 5 -> 5; matrix products, arithmetic and copies ran while one was open for 0% -> 4% of each run, Pallas kernels for 0% -> 0%
where the time goes in v1:
time: 458 us; the launch traced here: 457 us
  waiting for transfers between devices  249 us (54%)
  starting transfers between devices  72.7 us (16%)
  blocking collectives  62.9 us (14%)
  local copies, waits for them, and re-layouts  29.7 us (6%)
  matrix products  22.8 us (5%)
  between operations  13.4 us (3%)
  other arithmetic  6.74 us (1%)
    ppermute x3, waiting for transfers between devices, shards(): lax.ppermute(ring[-1], 'sp', [(dev, (dev + 1) % 4) for dev in range(4)])  200 us
    ppermute x3, starting transfers between devices, shards(): lax.ppermute(ring[-1], 'sp', [(dev, (dev + 1) % 4) for dev in range(4)])  72.6 us
    reduce_scatter x1, waiting for transfers between devices, shards(): lax.psum_scatter((jnp.dot(att_narrow, out_narrow, preferred_element_type=...  24.9 us
    reduce_scatter x1, waiting for transfers between devices, shards(): lax.psum_scatter(partials.astype(jnp.bfloat16), 'tp', scatter_dimension=0...  22.8 us
    unnamed x42, local copies, waits for them, and re-layouts  21.2 us
    all_gather x1, blocking collectives, attend(): wide_keys = lax.all_gather(key_wide, 'sp', axis=0, tiled=True)  17.7 us
    all_gather x1, blocking collectives, attend(): narrow_values = lax.all_gather(value_narrow, 'sp', axis=0, tiled=True)  15.7 us
    all_gather x1, blocking collectives, attend(): wide_values = lax.all_gather(value_wide, 'sp', axis=0, tiled=True)  15.3 us
  transfers between devices with their start and end apart: 7, of which 5 were waited for; matrix products, arithmetic and copies ran while one was open for 4% of the time, Pallas kernels for 0%

profile of v1, /device:TPU:0, one launch (start us, length us, event | category | flops | bytes accessed | tf_op | source)
XLA Modules:
  0.0 457.2 jit_solution(2606042599777396389)
XLA Ops:
  6.6 17.7 %all_gather.20 = bf16[1024,1,256]{2,0,1:T(8,128)(2,1)S(1)} all-gather(bf16[256,1,256]{2,0,1:T(8,128)(2,1)} %param.24), channel_id=1, replica_groups=mesh['grp'=2,'sp'=4,'tp'=4] {'sp'}, dimensions={0}, use_global_device_ids=true | all-gather | bytes 655360 | tf_op jit(solution)/shard_map/all_gather | solution.py:91
  24.3 0.1 reshape.256
  24.4 1.1 copy.33
  25.5 0.2 copy.35
  25.7 15.3 %all_gather.21 = bf16[1024,1,128]{2,0,1:T(8,128)(2,1)} all-gather(bf16[256,1,128]{2,0,1:T(8,128)(2,1)S(1)} %copy-done.12), channel_id=1, replica_groups=mesh['grp'=2,'sp'=4,'tp'=4] {'sp'}, dimensions={0}, use_global_device_ids=true | all-gather | bytes 327680 | tf_op jit(solution)/shard_map/all_gather | solution.py:92
  41.1 8.2 %while.31 = (s32[]{:T(128)}, f32[1,2,2,256]{3,1,2,0:T(2,128)S(1)}, f32[1,2,2,256]{3,1,2,0:T(2,128)S(1)}, f32[1,2,2,256,128]{4,3,2,1,0:T(8,128)}, bf16[2,512,1,2,...) while((s32[]{:T(128)}, f32[1,2,2,256]{3,1,2,0:T(2,128)S(1)}, ...), condition=%wide.region_8.9_spmd.clone, body=%wide.region_5.0_spmd.clone.sunk | while | flops 271980544 | bytes 13832389 | solution.py:53
  41.1 0.2 constant_dynamic-slice_fusion.2
  41.3 0.6 copy-done.4
  41.9 0.4 bitcast_reduce_fusion.5
  42.4 0.4 fusion.83
  42.8 0.5 copy-done.9
  43.3 1.3 fusion.84
  44.7 0.2 constant_dynamic-slice_fusion.2
  44.9 0.6 copy-done.4
  45.5 0.4 bitcast_reduce_fusion.5
  46.0 0.4 fusion.83
  46.4 0.5 copy-done.9
  46.9 2.3 fusion.84
  49.3 0.6 slice_bitcast_fusion.5
  49.9 14.2 %all_gather.18 = bf16[1024,1,128]{2,0,1:T(8,128)(2,1)S(1)} all-gather(bf16[256,1,128]{2,0,1:T(8,128)(2,1)S(1)} %copy-done.13), channel_id=1, replica_groups=mesh['grp'=2,'sp'=4,'tp'=4] {'sp'}, dimensions={0}, use_global_device_ids=true | all-gather | bytes 327680 | tf_op jit(solution)/shard_map/all_gather | solution.py:89
  64.0 0.2 reshape.272
  64.3 0.4 copy.29
  64.7 15.7 %all_gather.19 = bf16[1024,1,128]{2,0,1:T(8,128)(2,1)} all-gather(bf16[256,1,128]{2,0,1:T(8,128)(2,1)} %param.22), channel_id=1, replica_groups=mesh['grp'=2,'sp'=4,'tp'=4] {'sp'}, dimensions={0}, use_global_device_ids=true | all-gather | bytes 327680 | tf_op jit(solution)/shard_map/all_gather | solution.py:90
  80.3 0.1 copy.28
  80.5 6.7 %while.30 = (s32[]{:T(128)}, f32[1,2,2,256]{3,1,2,0:T(2,128)S(1)}, f32[1,2,2,256]{3,1,2,0:T(2,128)S(1)}, f32[1,2,2,256,128]{4,3,2,1,0:T(8,128)}, bf16[2,512,1,2,...) while((s32[]{:T(128)}, f32[1,2,2,256]{3,1,2,0:T(2,128)S(1)}, ...), condition=%wide.region_3.4_spmd.clone, body=%wide.region_0.3_spmd.clone.sunk | while | flops 204871680 | bytes 8851597 | solution.py:53
  80.5 0.5 bitcast_reduce_fusion.4
  81.0 0.4 fusion.78
  81.4 0.5 copy-done.10
  82.0 1.3 fusion.79
  83.3 0.5 bitcast_reduce_fusion.4
  83.8 0.4 fusion.78
  84.3 0.5 copy-done.10
  84.8 2.3 fusion.79
  87.2 1.2 copy.36
  88.4 1.2 copy.31
  89.7 0.2 multiply_reduce_fusion
  90.0 0.1 multiply_convert_fusion
  90.1 0.5 fusion.58
  90.5 0.6 copy-done.8
  91.1 1.5 fusion.35
  92.6 0.0 all-gather.3.cloned.1.call-start
  92.7 24.9 %reduce-scatter.3.cloned.1.call-done = bf16[64,2048]{1,0:T(8,128)(2,1)} async-done(((bf16[256,2048]{1,0:T(8,128)(2,1)}), bf16[64,2048]{1,0:T(8,128)(2,1)}) %reduce-scatter.3.cloned.1.call-update) | async-done | bytes 262160 | tf_op jit(solution)/shard_map/reduce_scatter | solution.py:129
  117.6 1.1 fusion.41
  118.8 1.8 fusion.43
  120.6 0.0 all-gather.5.cloned.1.call-start
  120.6 0.7 all-gather.5.cloned.1.call-update
  121.4 1.6 collective-permute-start
  122.9 66.2 %collective-permute-done = bf16[512,2048]{1,0:T(8,128)(2,1)S(1)} collective-permute-done((bf16[512,2048]{1,0:T(8,128)(2,1)S(1)}, bf16[512,2048]{1,0:T(8,128)(2,1)S(1)}, u32[]{:S(2)}, u32[]{:S(2)}) %collective-permute-start) | collective-permute-done | bytes 2097184 | tf_op jit(solution)/shard_map/ppermute | solution.py:147
  189.1 1.4 copy-done.2
  190.5 21.8 %collective-permute-start.1 = (bf16[512,2048]{1,0:T(8,128)(2,1)S(1)}, bf16[512,2048]{1,0:T(8,128)(2,1)}, u32[]{:S(2)}, u32[]{:S(2)}) collective-permute-start(bf16[512,2048]{1,0:T(8,128)(2,1)S(1)} %collective-permute-done), channel_id=1, source_target_pairs={{0,4},{4,8},{8,12},{12,0},{1,5},{5,9},{9,13},{13,1},{2,6},{6,10},{... | collective-permute-start | bytes 6291464 | tf_op jit(solution)/shard_map/ppermute | solution.py:147
  212.3 88.8 %collective-permute-done.1 = bf16[512,2048]{1,0:T(8,128)(2,1)} collective-permute-done((bf16[512,2048]{1,0:T(8,128)(2,1)S(1)}, bf16[512,2048]{1,0:T(8,128)(2,1)}, u32[]{:S(2)}, u32[]{:S(2)}) %collective-permute-start.1) | collective-permute-done | bytes 2097184 | tf_op jit(solution)/shard_map/ppermute | solution.py:147
  301.1 49.2 %collective-permute-start.2 = (bf16[512,2048]{1,0:T(8,128)(2,1)}, bf16[512,2048]{1,0:T(8,128)(2,1)}, u32[]{:S(2)}, u32[]{:S(2)}) collective-permute-start(bf16[512,2048]{1,0:T(8,128)(2,1)} %collective-permute-done.1), channel_id=1, source_target_pairs={{0,4},{4,8},{8,12},{12,0},{1,5},{5,9},{9,13},{13,1},{2,6},{6,10},{... | collective-permute-start | bytes 6291464 | tf_op jit(solution)/shard_map/ppermute | solution.py:147
  350.3 45.3 %collective-permute-done.2 = bf16[512,2048]{1,0:T(8,128)(2,1)} collective-permute-done((bf16[512,2048]{1,0:T(8,128)(2,1)}, bf16[512,2048]{1,0:T(8,128)(2,1)}, u32[]{:S(2)}, u32[]{:S(2)}) %collective-permute-start.2) | collective-permute-done | bytes 2097184 | tf_op jit(solution)/shard_map/ppermute | solution.py:147
  395.6 3.2 constant_dynamic-update-slice_fusion.7
  398.8 3.3 constant_dynamic-update-slice_fusion.6
  402.1 1.5 constant_dynamic-update-slice_fusion.5
  403.6 1.5 constant_dynamic-update-slice_fusion.4
  405.1 3.2 constant_dynamic-update-slice_fusion.3
  408.3 3.2 constant_dynamic-update-slice_fusion.2
  411.5 1.5 constant_dynamic-update-slice_fusion.1
  413.0 1.4 constant_dynamic-update-slice_fusion
  414.4 11.7 %convolution_convert_fusion = bf16[256,2048]{1,0:T(8,128)(2,1)} fusion(bf16[2048,2048]{1,0:T(8,128)(2,1)} %all-gather.5.cloned.1.call-done, bf16[256,2048]{1,0:T(8,128)(2,1)} %all-gather.3.cloned.1.call-done, bf16[4096,2048]{1,0:T(8,128)(2,1)} %constant_dynamic-update-slice_fusion, s32[]{:T(128)S(6)} %select_n.14), kind=kOutput, calls=%fused_computation.54 | convolution fusion | flops 4297064448 | bytes 18874372 | tf_op jit(solution)/shard_map/dot_general | solution.py:153
  426.1 22.8 %reduce-scatter.5.cloned.1.call-done = bf16[64,2048]{1,0:T(8,128)(2,1)} async-done(((bf16[256,2048]{1,0:T(8,128)(2,1)}), bf16[64,2048]{1,0:T(8,128)(2,1)}) %reduce-scatter.5.cloned.1.call-update) | async-done | bytes 262160 | tf_op jit(solution)/shard_map/reduce_scatter | solution.py:158
  448.9 1.7 fusion.44
  (73 shorter events, 0.4 us)
Async XLA Ops:
  6.5 83.5 %copy-start = (bf16[256,2048]{1,0:T(8,128)(2,1)S(1)}, bf16[256,2048]{1,0:T(8,128)(2,1)}, u32[]{:S(2)}) copy-start(bf16[256,2048]{1,0:T(8,128)(2,1)} %param.29) | copy-start | bytes 3145732
  6.5 19.2 %copy-start.12 = (bf16[256,1,128]{2,0,1:T(8,128)(2,1)S(1)}, bf16[256,1,128]{2,0,1:T(8,128)(2,1)}, u32[]{:S(2)}) copy-start(bf16[256,1,128]{2,0,1:T(8,128)(2,1)} %param.25) | copy-start | bytes 196612
  6.5 111.1 %reduce-scatter.3.cloned.1.call-start = ((), (), s32[]{:S(2)}) async-start(), calls=%async_computation.2 | async-start | bytes 1310720 | tf_op jit(solution)/shard_map/reduce_scatter | solution.py:129
  41.1 8.8 %copy-start.13 = (bf16[256,1,128]{2,0,1:T(8,128)(2,1)S(1)}, bf16[256,1,128]{2,0,1:T(8,128)(2,1)}, u32[]{:S(2)}) copy-start(bf16[256,1,128]{2,0,1:T(8,128)(2,1)} %param.21) | copy-start | bytes 196612
  41.1 0.8 copy-start.4
  42.4 1.0 copy-start.9
  42.8 1.8 copy-start.5
  44.7 0.8 copy-start.4
  45.9 1.0 copy-start.9
  46.4 2.9 copy-start.5
  49.3 31.1 %copy-start.11 = (bf16[256,2,128]{2,1,0:T(2,128)(2,1)S(1)}, bf16[256,2,128]{2,1,0:T(2,128)(2,1)}, u32[]{:S(2)}) copy-start(bf16[256,2,128]{2,1,0:T(2,128)(2,1)} %param.20) | copy-start | bytes 393220
  81.0 1.0 copy-start.10
  83.8 1.0 copy-start.10
  87.1 2.6 copy-start.14
  87.1 2.6 copy-start.16
  87.2 2.6 copy-start.17
  87.2 2.8 copy-start.18
  89.9 1.2 copy-start.8
  91.1 1.5 copy-start.15
  91.1 26.5 %copy-start.6 = (bf16[64,2048]{1,0:T(8,128)(2,1)S(1)}, bf16[64,2048]{1,0:T(8,128)(2,1)}, u32[]{:S(2)}) copy-start(bf16[64,2048]{1,0:T(8,128)(2,1)} %param.19) | copy-start | bytes 786436
  92.6 28.7 %copy-start.1 = (bf16[512,2048]{1,0:T(8,128)(2,1)S(1)}, bf16[512,2048]{1,0:T(8,128)(2,1)}, u32[]{:S(2)}) copy-start(bf16[512,2048]{1,0:T(8,128)(2,1)} %param.32) | copy-start | bytes 6291460
  92.6 321.8 %all-gather.3.cloned.1.call-start = ((), (), s32[]{:S(2)}) async-start(), calls=%async_computation.3 | async-start | bytes 1310720 | tf_op jit(solution)/shard_map/all_gather | solution.py:144
  120.6 293.8 %all-gather.5.cloned.1.call-start = ((), (), s32[]{:S(2)}) async-start(), calls=%async_computation.4 | async-start | bytes 10485760 | tf_op jit(solution)/shard_map/all_gather | solution.py:155
  121.3 327.6 %reduce-scatter.5.cloned.1.call-start = ((), (), s32[]{:S(2)}) async-start(), calls=%async_computation.5 | async-start | bytes 1310720 | tf_op jit(solution)/shard_map/reduce_scatter | solution.py:158
  121.4 67.8 %collective-permute-start = (bf16[512,2048]{1,0:T(8,128)(2,1)S(1)}, bf16[512,2048]{1,0:T(8,128)(2,1)S(1)}, u32[]{:S(2)}, u32[]{:S(2)}) collective-permute-start(bf16[512,2048]{1,0:T(8,128)(2,1)S(1)} %copy-done.1), channel_id=1, source_target_pairs={{0,4},{4,8},{8,12},{12,0},{1,5},{5,9},{9,13},{13,1},{2,6},{6,10},{... | collective-permute-start | bytes 6291464 | tf_op jit(solution)/shard_map/ppermute | solution.py:147
  189.1 1.4 copy-start.2
  190.5 110.6 %collective-permute-start.1 = (bf16[512,2048]{1,0:T(8,128)(2,1)S(1)}, bf16[512,2048]{1,0:T(8,128)(2,1)}, u32[]{:S(2)}, u32[]{:S(2)}) collective-permute-start(bf16[512,2048]{1,0:T(8,128)(2,1)S(1)} %collective-permute-done), channel_id=1, source_target_pairs={{0,4},{4,8},{8,12},{12,0},{1,5},{5,9},{9,13},{13,1},{2,6},{6,10},{... | collective-permute-start | bytes 6291464 | tf_op jit(solution)/shard_map/ppermute | solution.py:147
  301.1 94.5 %collective-permute-start.2 = (bf16[512,2048]{1,0:T(8,128)(2,1)}, bf16[512,2048]{1,0:T(8,128)(2,1)}, u32[]{:S(2)}, u32[]{:S(2)}) collective-permute-start(bf16[512,2048]{1,0:T(8,128)(2,1)} %collective-permute-done.1), channel_id=1, source_target_pairs={{0,4},{4,8},{8,12},{12,0},{1,5},{5,9},{9,13},{13,1},{2,6},{6,10},{... | collective-permute-start | bytes 6291464 | tf_op jit(solution)/shard_map/ppermute | solution.py:147
  398.8 3.3 copy-start.3
  414.4 34.5 %copy-start.7 = (bf16[64,2048]{1,0:T(8,128)(2,1)S(1)}, bf16[64,2048]{1,0:T(8,128)(2,1)}, u32[]{:S(2)}) copy-start(bf16[64,2048]{1,0:T(8,128)(2,1)} %reduce-scatter.3.cloned.1.call-done) | copy-start | bytes 786436
Sparse Core Ops, SparseCore 0:
  92.7 24.8 reduce-scatter.2
  120.7 16.7 all-gather.2
  139.0 214.4 all-gather.4
  426.2 22.6 reduce-scatter.4
